TPU v7x, 32 devices: a whole 2x2x4 slice. The times are simulated.
32 devices in a mesh: sp: 8 (over z, y), tp: 4 (over x, core).
Axes of the slice: x: 2, y: 2, z: 4, core: 2. Of those that a mesh axis runs over, the one named last changes fastest.
Arguments:
- inputs: bfloat16 [12288, 2048], P('sp'), may hold values from -6 to 6
- norm_gain: float32 [2048], replicated, may hold values from 0.1 to 1.9
- pool_weight: bfloat16 [2048, 1024], P(None, 'tp'), may hold values from -0.125 to 0.125
- query_weight: bfloat16 [2048, 1024], P(None, 'tp'), may hold values from -0.125 to 0.125
- forget_weight: bfloat16 [2048, 1024], P(None, 'tp'), may hold values from -0.125 to 0.125
- value_weight: bfloat16 [2048, 1024], P(None, 'tp'), may hold values from -0.125 to 0.125
- outgate_weight: bfloat16 [2048, 1024], P(None, 'tp'), may hold values from -0.125 to 0.125
- pool_mix: bfloat16 [4, 256, 256], P('tp'), may hold values from -0.375 to 0.375
- pool_scale: float32 [1024], P('tp'), may hold values from 0.1 to 1.9
- lower_bound: float32 [1024], P('tp'), may hold values from 0.9 to 1
- extra_decay: float32 [12288, 8], P('sp', 'tp'), may hold values from -1 to 0
- recur_gain: float32 [1024], P('tp'), may hold values from 0.1 to 1.9
- init_state: float32 [8, 128, 128], P('tp'), may hold values from -0.013531647 to 0.013531647
- out_pool: bfloat16 [1024, 2048], P('tp'), may hold values from -0.125 to 0.125
- out_recur: bfloat16 [1024, 2048], P('tp'), may hold values from -0.125 to 0.125
Outputs:
- mixed: bfloat16 [12288, 2048], P(('sp', 'tp'))
All inputs are finite; a program needn't handle non-finite values.
Results may differ from a plain program's by a relative error of at most 0.014.
Values may be sent and summed in bfloat16 or wider, within the bound.
A program may use at most 128 MiB of HBM per device.

v0:
```python
import functools
import jax
import jax.numpy as jnp
from jax import lax
from jax.experimental import pallas as pl
from jax.experimental.pallas import tpu as pltpu
from jax.sharding import PartitionSpec as P

NORM_EPS = 1e-05
HALO = 16
CHUNK = 128
BF = jnp.bfloat16
F32 = jnp.float32
VMEM_LIMIT = 60 * 1024 * 1024


def pick_tile(rows):
    for tile in (256, 128):
        if rows % tile == 0:
            return tile
    return rows


def dot(a, b, dims=((1,), (0,))):
    return lax.dot_general(a, b, (dims, ((), ())), preferred_element_type=F32)


def log1m(k):
    acc = jnp.full_like(k, 1.0 / 9.0)
    for n in range(8, 0, -1):
        acc = acc * k + 1.0 / n
    return -k * acc


def sigmoid(x):
    return 1.0 / (1.0 + jnp.exp(-x))


def front_kernel(
    x_ref, gain_ref, wp_ref, wq_ref, wf_ref, wv_ref, wo_ref, lb_ref, extra_ref,
    pool_ref, rl_ref, qc_ref, og_ref, tot_ref, st_ref,
    run_ref,
):
    step = pl.program_id(0)
    heads, hk = st_ref.shape[0], st_ref.shape[1]

    @pl.when(step == 0)
    def _():
        st_ref[...] = jnp.zeros_like(st_ref)
        run_ref[...] = jnp.zeros_like(run_ref)

    x = x_ref[...].astype(F32)
    scale = lax.rsqrt(jnp.mean(x * x, axis=-1, keepdims=True) + NORM_EPS)
    normed = (x * scale * gain_ref[...]).astype(BF)
    pool_ref[...] = dot(normed, wp_ref[...]).astype(BF)
    og_ref[...] = dot(normed, wo_ref[...]).astype(BF)
    q_raw = dot(normed, wq_ref[...])
    f_raw = dot(normed, wf_ref[...])
    value = dot(normed, wv_ref[...]).astype(BF)
    gap = 1.0 - lb_ref[...]
    q_in = q_raw * sigmoid(q_raw)
    k_in = gap * sigmoid(-f_raw)
    extra = extra_ref[...]
    rows = x.shape[0]
    log_f = log1m(k_in) + jnp.concatenate(
        [jnp.broadcast_to(extra[:, h : h + 1], (rows, hk)) for h in range(heads)], axis=1
    )
    chunk = min(CHUNK, rows)
    t_idx = lax.broadcasted_iota(jnp.int32, (chunk, chunk), 0)
    s_idx = lax.broadcasted_iota(jnp.int32, (chunk, chunk), 1)
    causal = t_idx >= s_idx
    tril = causal.astype(F32).astype(BF)
    for c in range(rows // chunk):
        r = slice(c * chunk, (c + 1) * chunk)
        lf = log_f[r]
        hi = lf.astype(BF)
        lo = (lf - hi.astype(F32)).astype(BF)
        cum = dot(tril, hi) + dot(tril, lo)
        mid = cum[chunk // 2 - 1 : chunk // 2]
        last = cum[chunk - 1 : chunk]
        run = run_ref[...]
        e1 = jnp.exp(cum - mid)
        q_rel = q_in[r] * e1
        k_rel = k_in[r] * jnp.exp(mid - cum)
        q_start = q_rel * jnp.exp(mid)
        k_end = (k_rel * jnp.exp(last - mid)).astype(BF)
        decay = jnp.exp(last)
        qc_ref[r, :] = (q_start * jnp.exp(run)).astype(BF)
        run_ref[...] = run + last
        q_rel = q_rel.astype(BF)
        k_rel = k_rel.astype(BF)
        q_start = q_start.astype(BF)
        for h in range(heads):
            cols = slice(h * hk, (h + 1) * hk)
            vv = value[r, cols]
            scores = dot(q_rel[:, cols], k_rel[:, cols], ((1,), (1,)))
            scores = jnp.where(causal, scores, 0.0).astype(BF)
            st = st_ref[h]
            rl_ref[r, cols] = dot(scores, vv) + dot(q_start[:, cols], st.astype(BF), ((1,), (1,)))
            st_ref[h] = st * decay[:, cols] + dot(vv, k_end[:, cols], ((0,), (0,)))
    tot_ref[...] = run_ref[...]


def back_kernel(
    idx_ref, pool_ref, rl_ref, qc_ref, og_ref, halo_ref, tots_ref, sts_ref, init_ref, rgain_ref,
    mix_ref, pscale_ref,
    y_ref,
    st_ref, prev_ref,
):
    step = pl.program_id(0)
    heads, hk = init_ref.shape[0], init_ref.shape[1]
    me, group = idx_ref[0], idx_ref[1]
    rows, width = pool_ref.shape

    @pl.when(step == 0)
    def _():
        prev_ref[...] = halo_ref[...]
        for h in range(heads):
            st_ref[h] = init_ref[h].T

        @pl.loop(0, me)
        def _(k):
            for h in range(heads):
                decay = jnp.exp(tots_ref[k, :, h * hk : (h + 1) * hk])
                st_ref[h] = st_ref[h] * decay + sts_ref[k, h].astype(F32)

    groups, gw = mix_ref.shape[0], mix_ref.shape[1]
    pool_in = pool_ref[...]
    prev = prev_ref[...]
    t_idx = lax.broadcasted_iota(jnp.int32, (rows, rows), 0)
    s_idx = lax.broadcasted_iota(jnp.int32, (rows, rows), 1)
    tp_idx = lax.broadcasted_iota(jnp.int32, (rows, HALO), 0)
    sp_idx = lax.broadcasted_iota(jnp.int32, (rows, HALO), 1)
    pos = (me * pl.num_programs(0) + step) * rows + lax.broadcasted_iota(jnp.int32, (rows, 1), 0)
    for g in range(groups):
        window = jnp.int32(2) << (group * groups + g)
        cols = slice(g * gw, (g + 1) * gw)
        band = jnp.where((t_idx >= s_idx) & (t_idx - s_idx < window), 1.0, 0.0).astype(BF)
        band_prev = jnp.where(tp_idx + HALO - sp_idx < window, 1.0, 0.0).astype(BF)
        total = dot(band, pool_in[:, cols]) + dot(band_prev, prev[:, cols])
        reach = jnp.minimum(pos + 1, window).astype(F32)
        pooled = (total / reach - pool_in[:, cols].astype(F32)).astype(BF)
        y_ref[:, cols] = (dot(pooled, mix_ref[g]) * pscale_ref[:, cols]).astype(BF)
    prev_ref[...] = pool_in[rows - HALO :]
    out_gate = og_ref[...].astype(F32)
    gate = out_gate * sigmoid(out_gate) * rgain_ref[...]
    for h in range(heads):
        cols = slice(h * hk, (h + 1) * hk)
        rec = rl_ref[:, cols] + dot(qc_ref[:, cols], st_ref[h].astype(BF), ((1,), (1,)))
        rec = rec * lax.rsqrt(jnp.mean(rec * rec, axis=-1, keepdims=True) + NORM_EPS)
        y_ref[:, width + h * hk : width + (h + 1) * hk] = (rec * gate[:, cols]).astype(BF)


def per_device(
    inputs, norm_gain, pool_weight, query_weight, forget_weight, value_weight, outgate_weight,
    pool_mix, pool_scale, lower_bound, extra_decay, recur_gain, init_state, out_pool, out_recur,
):
    rows, d = inputs.shape
    width = pool_weight.shape[1]
    rwidth = query_weight.shape[1]
    heads, hk = init_state.shape[0], init_state.shape[1]
    tile = pick_tile(rows)
    steps = rows // tile
    w_out = lax.all_gather(jnp.concatenate([out_pool, out_recur], axis=0), "tp", axis=0, tiled=True)

    def rowed(w):
        return pl.BlockSpec((tile, w), lambda i: (i, 0))

    def whole(*shape):
        return pl.BlockSpec(shape, lambda i: (0,) * len(shape))

    params = pltpu.CompilerParams(
        dimension_semantics=("arbitrary",), vmem_limit_bytes=VMEM_LIMIT
    )
    pool_in, rl, qc, og, tot, st = pl.pallas_call(
        front_kernel,
        grid=(steps,),
        in_specs=[rowed(d), whole(1, d), whole(d, width)]
        + [whole(d, rwidth)] * 4
        + [whole(1, rwidth), rowed(heads)],
        out_specs=[rowed(width), rowed(rwidth), rowed(rwidth), rowed(rwidth), whole(1, rwidth), whole(heads, hk, hk)],
        out_shape=[
            jax.ShapeDtypeStruct((rows, width), BF),
            jax.ShapeDtypeStruct((rows, rwidth), F32),
            jax.ShapeDtypeStruct((rows, rwidth), BF),
            jax.ShapeDtypeStruct((rows, rwidth), BF),
            jax.ShapeDtypeStruct((1, rwidth), F32),
            jax.ShapeDtypeStruct((heads, hk, hk), F32),
        ],
        scratch_shapes=[pltpu.VMEM((1, rwidth), F32)],
        compiler_params=params,
        cost_estimate=pl.CostEstimate(
            flops=2 * rows * d * (width + 4 * rwidth), bytes_accessed=2 * rows * d, transcendentals=0
        ),
    )(
        inputs, norm_gain[None], pool_weight, query_weight, forget_weight, value_weight,
        outgate_weight, lower_bound[None], extra_decay,
    )
    n = lax.axis_size("sp")
    halo = lax.ppermute(pool_in[rows - HALO :], "sp", [(i, i + 1) for i in range(n - 1)])
    tots = lax.all_gather(tot, "sp")
    sts = lax.all_gather(st.astype(BF), "sp")
    idx = jnp.stack([lax.axis_index("sp"), lax.axis_index("tp")]).astype(jnp.int32)
    y = pl.pallas_call(
        back_kernel,
        grid=(steps,),
        in_specs=[
            pl.BlockSpec(memory_space=pltpu.SMEM),
            rowed(width), rowed(rwidth), rowed(rwidth), rowed(rwidth),
            whole(HALO, width), whole(n, 1, rwidth), whole(n, heads, hk, hk), whole(heads, hk, hk),
            whole(1, rwidth), whole(*pool_mix.shape), whole(1, width),
        ],
        out_specs=rowed(width + rwidth),
        out_shape=jax.ShapeDtypeStruct((rows, width + rwidth), BF),
        scratch_shapes=[pltpu.VMEM((heads, hk, hk), F32), pltpu.VMEM((HALO, width), BF)],
        compiler_params=params,
        cost_estimate=pl.CostEstimate(
            flops=2 * rows * width * width * 2, bytes_accessed=8 * rows * width, transcendentals=0
        ),
    )(idx, pool_in, rl, qc, og, halo, tots, sts, init_state, recur_gain[None], pool_mix, pool_scale[None])
    seen = lax.all_to_all(y, "tp", split_axis=0, concat_axis=1, tiled=True)
    return jnp.dot(seen, w_out, preferred_element_type=F32).astype(BF)


def solution(mesh):
    in_specs = (
        P("sp", None), P(), P(None, "tp"), P(None, "tp"), P(None, "tp"), P(None, "tp"),
        P(None, "tp"), P("tp", None, None), P("tp"), P("tp"), P("sp", "tp"), P("tp"),
        P("tp", None, None), P("tp", None), P("tp", None),
    )
    return jax.shard_map(
        per_device, mesh=mesh, in_specs=in_specs, out_specs=P(("sp", "tp"), None), check_vma=False
    )
```

profile of v0, /device:TPU:0, one launch (start us, length us, event | category | flops | bytes accessed | tf_op | source)
XLA Modules:
  0.0 140.2 jit_solution(6224285328981351746)
XLA Ops:
  6.5 0.0 all-gather.5.cloned.1.call-start
  6.5 3.1 %pad_maximum_fusion = bf16[512,2048]{1,0:T(8,128)(2,1)} fusion(bf16[256,2048]{1,0:T(8,128)(2,1)} %param.29, bf16[256,2048]{1,0:T(8,128)(2,1)} %param.28), kind=kLoop, calls=%fused_computation.1 | loop fusion | flops 4194304 | bytes 4194304 | tf_op jit(solution)/shard_map/concatenate | solution.py:164
  9.7 0.0 copy-start
  9.7 0.0 all-gather.5.cloned.1.call-update
  9.7 0.7 copy-done
  10.4 1.2 copy.19.extra_ref
  11.6 21.9 %shard_map.145 = (bf16[1536,256]{1,0:T(8,128)(2,1)}, f32[1536,256]{1,0:T(8,128)}, bf16[1536,256]{1,0:T(8,128)(2,1)}, bf16[1536,256]{1,0:T(8,128)(2,1)}, f32[1,256]{1,0:T(1,128)}, /*index=5*/f32[2,128,128]{2,1,0:T(8,128)}) custom-call(bf16[1536,2048]{1,0:T(8,128)(2,1)} %x_ref.1, f32[1,2048]{1,0:T(1,128)} %bitcast.20, bf16[2048,256]{1,0:T(8,128)(2,1)} %wp_ref.1, ...), custom_call_target="tpu_custom_call" | custom-call | flops 8053063680 | bytes 6291456 | tf_op jit(solution)/shard_map/pallas_call | solution.py:175
  33.4 0.7 slice.3
  34.1 4.9 %collective-permute-start = (bf16[16,256]{1,0:T(8,128)(2,1)S(1)}, bf16[16,256]{1,0:T(8,128)(2,1)S(1)}, u32[]{:S(2)}, u32[]{:S(2)}) collective-permute-start(bf16[16,256]{1,0:T(8,128)(2,1)S(1)} %slice.3), channel_id=1, source_target_pairs={{0,4},{4,8},{8,12},{12,16},{16,20},{20,24},{24,28},{1,5},{5,9},{9,... | collective-permute-start | bytes 24584 | tf_op jit(solution)/shard_map/ppermute | solution.py:200
  39.0 0.9 convert_element_type.6
  40.0 33.8 %all-gather.1 = bf16[16,128,128]{2,1,0:T(8,128)(2,1)} all-gather(bf16[2,128,128]{2,1,0:T(8,128)(2,1)S(1)} %convert_element_type.6), channel_id=3, replica_groups=mesh['sp'=8,'tp'=4] {'sp'}, dimensions={0}, use_global_device_ids=true | all-gather | bytes 589824 | tf_op jit(solution)/shard_map/all_gather | solution.py:202
  73.8 0.6 pad_add_fusion.idx_ref
  74.4 18.8 %all-gather.2.tots_ref = f32[8,1,256]{2,1,0:T(1,128)} all-gather(f32[1,1,256]{2,1,0:T(1,128)} %bitcast.19), channel_id=2, replica_groups=mesh['sp'=8,'tp'=4] {'sp'}, dimensions={0}, use_global_device_ids=true | all-gather | bytes 9216 | tf_op jit(solution)/shard_map/all_gather | solution.py:201
  93.2 0.0 collective-permute-done.halo_ref
  93.2 0.0 copy-start.1
  93.2 0.6 copy-done.1
  93.8 7.0 %shard_map.146 = bf16[1536,512]{1,0:T(8,128)(2,1)} custom-call(s32[2]{0:T(128)} %pad_add_fusion.idx_ref, bf16[1536,256]{1,0:T(8,128)(2,1)} %get-tuple-element.11.pool_ref, f32[1536,256]{1,0:T(8,128)} %get-tuple-element.12.rl_ref, bf16[1536,256]{1,0:T(8,128)(2,1)} %get-tuple-element.13.qc_ref, bf16[1536,256]{1,0:T(8,128)(2,1)} %get-tuple-element.14.og_ref, ...), custom_call_target="tpu_custom_call" | custom-call | flops 402653184 | bytes 3145728 | tf_op jit(solution)/shard_map/pallas_call | solution.py:204
  100.8 1.9 %copy.20 = bf16[4,384,512]{1,2,0:T(8,128)(2,1)S(1)} copy(bf16[4,384,512]{2,1,0:T(8,128)(2,1)} %bitcast.14) | data formatting | bytes 3145728 | tf_op jit(solution)/shard_map/all_to_all | solution.py:221
  102.7 22.6 %all_to_all.19 = bf16[4,384,512]{1,2,0:T(8,128)(2,1)S(1)} all-to-all(bf16[4,384,512]{1,2,0:T(8,128)(2,1)S(1)} %copy.20), channel_id=1, replica_groups=mesh['sp'=8,'tp'=4] {'tp'}, dimensions={0} | all-to-all | bytes 3145728 | tf_op jit(solution)/shard_map/all_to_all | solution.py:221
  125.3 0.0 all-gather.5.cloned.1.call-done
  125.3 8.0 %convolution_convert_fusion = bf16[384,2048]{1,0:T(8,128)(2,1)} fusion(bf16[384,2048]{0,1:T(8,128)(2,1)S(1)} %bitcast.16, bf16[2048,2048]{1,0:T(8,128)(2,1)} %all-gather.5.cloned.1.call-done), kind=kOutput, calls=%fused_computation | convolution fusion | flops 3222011904 | bytes 11534336 | tf_op jit(solution)/shard_map/dot_general | solution.py:222
Async XLA Ops:
  6.5 118.8 %all-gather.5.cloned.1.call-start = ((), (), s32[]{:S(2)}) async-start(), calls=%async_computation.1 | async-start | bytes 10485760 | tf_op jit(solution)/shard_map/all_gather | solution.py:164
  9.7 0.7 copy-start
  34.1 59.1 %collective-permute-start = (bf16[16,256]{1,0:T(8,128)(2,1)S(1)}, bf16[16,256]{1,0:T(8,128)(2,1)S(1)}, u32[]{:S(2)}, u32[]{:S(2)}) collective-permute-start(bf16[16,256]{1,0:T(8,128)(2,1)S(1)} %slice.3), channel_id=1, source_target_pairs={{0,4},{4,8},{8,12},{12,16},{16,20},{20,24},{24,28},{1,5},{5,9},{9,... | collective-permute-start | bytes 24584 | tf_op jit(solution)/shard_map/ppermute | solution.py:200
  93.2 0.6 copy-start.1
Sparse Core Ops, SparseCore 0:
  9.8 60.9 all-gather.4
where the time goes:
time: 141 us; the launch traced here: 140 us
  blocking collectives  75.2 us (53%)
  Pallas kernels  28.9 us (20%)
  between operations  13.4 us (10%)
  matrix products  8 us (6%)
  local copies, waits for them, and re-layouts  5.05 us (4%)
  starting transfers between devices  4.89 us (3%)
  other arithmetic  4.7 us (3%)
    all_gather x1, blocking collectives, per_device(): sts = lax.all_gather(st.astype(BF), 'sp')  33.8 us
    all_to_all x1, blocking collectives, per_device(): seen = lax.all_to_all(y, 'tp', split_axis=0, concat_axis=1, tiled=True)  22.6 us
    pallas_call x1, Pallas kernels, per_device(): pl.pallas_call(front_kernel, grid=(steps,), in_specs=[rowed(d), whole(1,...  21.9 us
    all_gather x1, blocking collectives, per_device(): tots = lax.all_gather(tot, 'sp')  18.8 us
    dot_general x1, matrix products, per_device(): return jnp.dot(seen, w_out, preferred_element_type=F32).astype(BF)  8 us
    pallas_call x1, Pallas kernels, per_device(): pl.pallas_call(back_kernel, grid=(steps,), in_specs=[pl.BlockSpec(memory_...  7 us
    ppermute x1, starting transfers between devices, per_device(): lax.ppermute(pool_in[rows - HALO:], 'sp', [(i, i + 1) for i in range(n -...  4.89 us
    concatenate x1, other arithmetic, per_device(): jnp.concatenate([out_pool, out_recur], axis=0)  3.15 us
  transfers between devices with their start and end apart: 2, of which 0 were waited for; matrix products, arithmetic and copies ran while one was open for 4% of the time, Pallas kernels for 21%

commit v1 on v0

v1 whole, which is shorter than its diff:
```python
import functools
import jax
import jax.numpy as jnp
from jax import lax
from jax.experimental import pallas as pl
from jax.experimental.pallas import tpu as pltpu
from jax.sharding import PartitionSpec as P

NORM_EPS = 1e-05
HALO = 16
CHUNK = 128
BF = jnp.bfloat16
F32 = jnp.float32
VMEM_LIMIT = 60 * 1024 * 1024


def dot(a, b, dims=((1,), (0,))):
    return lax.dot_general(a, b, (dims, ((), ())), preferred_element_type=F32)


def log1m(k):
    acc = jnp.full_like(k, 1.0 / 9.0)
    for n in range(8, 0, -1):
        acc = acc * k + 1.0 / n
    return -k * acc


def sigmoid(x):
    return 1.0 / (1.0 + jnp.exp(-x))


MESH = pl.DeviceIdType.MESH
PARTS = 4
SEM_D, SEM_X, SEM_F, SEM_Y, SEM_G, SEM_H, SEM_S, SEM_P, SEM_R = 0, 1, 5, 9, 13, 17, 18, 19, 22
SEMS = 25


def layer_kernel(
    n_sp, n_tp, steps,
    x_ref, gain_ref, wp_ref, wq_ref, wf_ref, wv_ref, wo_ref, lb_ref, extra_ref,
    tail_ref, op_ref, or_ref, init_ref, rgain_ref, mix_ref, pscale_ref,
    out_ref,
    run_ref, st_ref, rl_ref, qc_ref, og_ref, pin_ref, ypool_ref, yrec_ref, pgot_ref, rgot_ref,
    wg_ref, acc_ref, xhalo_ref, sbuf_ref, spair_ref, psend_ref, pgather_ref,
    send_sem, recv_sem, s2_send, s2_recv, loc_sem,
):
    step = pl.program_id(0)
    heads, hk = init_ref.shape[0], init_ref.shape[1]
    tile = x_ref.shape[0]
    gw = op_ref.shape[0]
    half = gw // PARTS
    n_pairs = n_sp // 2
    sp, tp = lax.axis_index("sp"), lax.axis_index("tp")
    hi_t, lo_t = tp // 2, tp % 2
    pair, par = sp // 2, sp % 2
    mate = hi_t * 2 + (1 - lo_t)
    cross = (1 - hi_t) * 2 + lo_t
    diag = (1 - hi_t) * 2 + (1 - lo_t)
    twin = pair * 2 + (1 - par)
    following = lax.rem(sp + 1, n_sp)

    def rdma(src, dst, sem, to):
        return pltpu.make_async_remote_copy(
            src_ref=src, dst_ref=dst, send_sem=send_sem.at[sem], recv_sem=recv_sem.at[sem],
            device_id=to, device_id_type=MESH,
        )

    def w_copy(slot, parity, c, sem, to):
        ref = wg_ref.at[slot, pl.ds(pl.multiple_of(parity * gw + c * half, half), half)]
        return rdma(ref, ref, sem + c, to)

    def copy_d():
        return rdma(wg_ref.at[tp], wg_ref.at[tp], SEM_D, (sp, mate))

    def copy_x(c):
        return w_copy(tp, par, c, SEM_X, (sp, cross))

    def copy_f(c):
        return w_copy(cross, par, c, SEM_F, (sp, mate))

    def copy_y(c):
        return w_copy(cross, par, c, SEM_Y, (twin, tp))

    def copy_g(c):
        return w_copy(cross, 1 - par, c, SEM_G, (sp, mate))

    def copy_h():
        return rdma(tail_ref, xhalo_ref, SEM_H, (following, tp))

    def copy_s():
        return rdma(sbuf_ref, spair_ref, SEM_S, (twin, tp))

    relations = (diag, cross, mate)

    def copy_p(r):
        return rdma(ypool_ref.at[relations[r]], pgot_ref.at[tp], SEM_P + r, (sp, relations[r]))

    def copy_r(r):
        return rdma(yrec_ref.at[relations[r]], rgot_ref.at[tp], SEM_R + r, (sp, relations[r]))

    def copy_2(k):
        to = lax.rem(pair + k, n_pairs)
        return pltpu.make_async_remote_copy(
            src_ref=psend_ref, dst_ref=pgather_ref.at[pair], send_sem=s2_send.at[k],
            recv_sem=s2_recv.at[pair], device_id=(to * 2 + par, tp), device_id_type=MESH,
        )

    def got_2(p):
        return pltpu.make_async_remote_copy(
            src_ref=psend_ref, dst_ref=pgather_ref.at[p], send_sem=s2_send.at[0],
            recv_sem=s2_recv.at[p], device_id=(p * 2 + par, tp), device_id_type=MESH,
        )

    def local_w():
        return (
            pltpu.make_async_copy(op_ref, wg_ref.at[tp, pl.ds(0, gw)], loc_sem.at[0]),
            pltpu.make_async_copy(or_ref, wg_ref.at[tp, pl.ds(gw, gw)], loc_sem.at[1]),
        )

    @pl.when(step == 0)
    def _():
        for copy in local_w():
            copy.start()
        barrier = pltpu.get_barrier_semaphore()
        for k in range(1, n_tp):
            pl.semaphore_signal(barrier, inc=1, device_id=(sp, lax.rem(tp + k, n_tp)), device_id_type=MESH)
        for k in range(1, n_sp):
            pl.semaphore_signal(barrier, inc=1, device_id=(lax.rem(sp + k, n_sp), tp), device_id_type=MESH)
        pl.semaphore_wait(barrier, n_tp - 1 + n_sp - 1)
        copy_h().start()
        for copy in local_w():
            copy.wait()
        for c in range(PARTS):
            copy_x(c).start()
        copy_d().start()
        st_ref[...] = jnp.zeros_like(st_ref)
        run_ref[...] = jnp.zeros_like(run_ref)

    def norm(x):
        x = x.astype(F32)
        scale = lax.rsqrt(jnp.mean(x * x, axis=-1, keepdims=True) + NORM_EPS)
        return (x * scale * gain_ref[...]).astype(BF)

    def pooling(index):
        base = pl.multiple_of(index * tile, HALO)
        rows = pin_ref[pl.ds(base, tile + HALO), :]
        t_idx = lax.broadcasted_iota(jnp.int32, (tile, tile + HALO), 0)
        j_idx = lax.broadcasted_iota(jnp.int32, (tile, tile + HALO), 1)
        back = t_idx + HALO - j_idx
        pos = (sp * steps + index) * tile + lax.broadcasted_iota(jnp.int32, (tile, 1), 0)
        groups, width = mix_ref.shape[0], mix_ref.shape[1]
        for g in range(groups):
            cols = slice(g * width, (g + 1) * width)
            group = tp * groups + g
            window = jnp.int32(2)
            for level in range(1, groups * n_tp):
                window = jnp.where(group >= level, 2 ** (level + 1), window)
            band = jnp.where((back >= 0) & (back < window), 1.0, 0.0).astype(BF)
            total = dot(band, rows[:, cols])
            reach = jnp.minimum(pos + 1, window).astype(F32)
            pooled = (total / reach - rows[HALO:, cols].astype(F32)).astype(BF)
            ypool_ref[index, :, cols] = (dot(pooled, mix_ref[g]) * pscale_ref[:, cols]).astype(BF)

    @pl.when(step == 1)
    def _():
        copy_h().wait_recv()
        halo = dot(norm(xhalo_ref[...]), wp_ref[...])
        pin_ref[0:HALO, :] = jnp.where(sp > 0, halo, 0.0).astype(BF)

    @pl.when(step > 0)
    def _():
        pooling(step - 1)

    normed = norm(x_ref[...])
    base = pl.multiple_of(step * tile, HALO)
    pin_ref[pl.ds(base + HALO, tile), :] = dot(normed, wp_ref[...]).astype(BF)
    og_ref[pl.ds(base, tile), :] = dot(normed, wo_ref[...]).astype(BF)
    q_raw = dot(normed, wq_ref[...])
    f_raw = dot(normed, wf_ref[...])
    value = dot(normed, wv_ref[...]).astype(BF)
    gap = 1.0 - lb_ref[...]
    q_in = q_raw * sigmoid(q_raw)
    k_in = gap * sigmoid(-f_raw)
    extra = extra_ref[...]
    log_f = log1m(k_in) + jnp.concatenate(
        [jnp.broadcast_to(extra[:, h : h + 1], (tile, hk)) for h in range(heads)], axis=1
    )
    chunk = CHUNK
    t_idx = lax.broadcasted_iota(jnp.int32, (chunk, chunk), 0)
    s_idx = lax.broadcasted_iota(jnp.int32, (chunk, chunk), 1)
    causal = t_idx >= s_idx
    tril = causal.astype(F32).astype(BF)
    for c in range(tile // chunk):
        r = slice(c * chunk, (c + 1) * chunk)
        there = pl.ds(pl.multiple_of(base + c * chunk, chunk), chunk)
        lf = log_f[r]
        hi = lf.astype(BF)
        lo = (lf - hi.astype(F32)).astype(BF)
        cum = dot(tril, hi) + dot(tril, lo)
        mid = cum[chunk // 2 - 1 : chunk // 2]
        last = cum[chunk - 1 : chunk]
        run = run_ref[...]
        e1 = jnp.exp(cum - mid)
        q_rel = q_in[r] * e1
        k_rel = k_in[r] * jnp.exp(mid - cum)
        q_start = q_rel * jnp.exp(mid)
        k_end = (k_rel * jnp.exp(last - mid)).astype(BF)
        decay = jnp.exp(last)
        qc_ref[there, :] = (q_start * jnp.exp(run)).astype(BF)
        run_ref[...] = run + last
        q_rel = q_rel.astype(BF)
        k_rel = k_rel.astype(BF)
        q_start = q_start.astype(BF)
        for h in range(heads):
            cols = slice(h * hk, (h + 1) * hk)
            vv = value[r, cols]
            scores = dot(q_rel[:, cols], k_rel[:, cols], ((1,), (1,)))
            scores = jnp.where(causal, scores, 0.0).astype(BF)
            st = st_ref[h]
            rl_ref[there, cols] = dot(scores, vv) + dot(q_start[:, cols], st.astype(BF), ((1,), (1,)))
            st_ref[h] = st * decay[:, cols] + dot(vv, k_end[:, cols], ((0,), (0,)))

    def relay_x(c):
        copy_x(c).wait_recv()
        copy_y(c).start()
        copy_f(c).start()

    for c in range(PARTS - 2):
        @pl.when(step == c + 1)
        def _():
            relay_x(c)

    def write_state(ref, h, decay, state):
        ref[h, 0:hk, :] = state.astype(BF)
        hi = decay.astype(BF).astype(F32)
        rows = jnp.concatenate([hi, decay - hi, jnp.zeros((14, hk), F32)], axis=0)
        ref[h, hk : hk + 16, :] = rows.astype(BF)

    def read_state(value):
        decay = value[hk : hk + 16].astype(F32)
        return decay[0:1] + decay[1:2], value[0:hk].astype(F32)

    @pl.when(step == steps - 1)
    def _():
        for h in range(heads):
            write_state(sbuf_ref, h, jnp.exp(run_ref[:, h * hk : (h + 1) * hk]), st_ref[h])
        copy_s().start()
        relay_x(PARTS - 2)
        pooling(steps - 1)
        for r in range(3):
            copy_p(r).start()
        pgot_ref[tp] = ypool_ref[tp]
        copy_s().wait_recv()
        odd = par == 1
        for h in range(heads):
            own = jnp.exp(run_ref[:, h * hk : (h + 1) * hk]), st_ref[h]
            other = read_state(spair_ref[h])
            early = jnp.where(odd, other[0], own[0]), jnp.where(odd, other[1], own[1])
            late = jnp.where(odd, own[0], other[0]), jnp.where(odd, own[1], other[1])
            write_state(psend_ref, h, early[0] * late[0], early[1] * late[0] + late[1])
        for k in range(1, n_pairs):
            @pl.when(pair + k < n_pairs)
            def _():
                copy_2(k).start()
        relay_x(PARTS - 1)
        for h in range(heads):
            st_ref[h] = init_ref[h].T
        for p in range(n_pairs - 1):
            @pl.when(p < pair)
            def _():
                got_2(p).wait_recv()
                for h in range(heads):
                    decay, state = read_state(pgather_ref[p, h])
                    st_ref[h] = st_ref[h] * decay + state
        for h in range(heads):
            decay, state = read_state(spair_ref[h])
            st_ref[h] = jnp.where(odd, st_ref[h] * decay + state, st_ref[h])

        def finish(index, ref, slot):
            rows = pl.ds(pl.multiple_of(index * tile, HALO), tile)
            out_gate = og_ref[rows, :].astype(F32)
            gate = out_gate * sigmoid(out_gate) * rgain_ref[...]
            for h in range(heads):
                cols = slice(h * hk, (h + 1) * hk)
                rec = rl_ref[rows, cols] + dot(qc_ref[rows, cols], st_ref[h].astype(BF), ((1,), (1,)))
                rec = rec * lax.rsqrt(jnp.mean(rec * rec, axis=-1, keepdims=True) + NORM_EPS)
                ref[slot, :, cols] = (rec * gate[:, cols]).astype(BF)

        for r in range(3):
            finish(relations[r], yrec_ref, relations[r])
            copy_r(r).start()
        finish(tp, rgot_ref, tp)
        for c in range(PARTS):
            copy_y(c).wait_recv()
            copy_g(c).start()
        copy_d().wait_recv()
        for c in range(PARTS):
            copy_f(c).wait_recv()
        for r in range(3):
            copy_p(r).wait_recv()
        for c in range(PARTS):
            copy_g(c).wait_recv()
        rwidth = rgot_ref.shape[2]
        span = min(512, out_ref.shape[1])
        parts_out = out_ref.shape[1] // span

        @pl.loop(0, parts_out)
        def _(j):
            cols = pl.ds(pl.multiple_of(j * span, span), span)
            acc = dot(pgot_ref[0], wg_ref[0, 0:gw, cols])
            for s in range(1, n_tp):
                acc = acc + dot(pgot_ref[s], wg_ref[s, 0:gw, cols])
            acc = acc + dot(rgot_ref[tp], wg_ref[tp, gw : gw + rwidth, cols])
            acc_ref[:, cols] = acc

        for r in range(2, -1, -1):
            copy_r(r).wait_recv()

        @pl.loop(0, parts_out)
        def _(j):
            cols = pl.ds(pl.multiple_of(j * span, span), span)
            acc = acc_ref[:, cols]
            for r in range(3):
                s = relations[r]
                acc = acc + dot(rgot_ref[s], wg_ref[s, gw : gw + rwidth, cols])
            out_ref[:, cols] = acc.astype(BF)

        copy_h().wait_send()
        copy_d().wait_send()
        copy_s().wait_send()
        for c in range(PARTS):
            copy_x(c).wait_send()
            copy_f(c).wait_send()
            copy_y(c).wait_send()
            copy_g(c).wait_send()
        for r in range(3):
            copy_p(r).wait_send()
            copy_r(r).wait_send()
        for k in range(1, n_pairs):
            @pl.when(pair + k < n_pairs)
            def _():
                copy_2(k).wait_send()


def per_device(
    inputs, norm_gain, pool_weight, query_weight, forget_weight, value_weight, outgate_weight,
    pool_mix, pool_scale, lower_bound, extra_decay, recur_gain, init_state, out_pool, out_recur,
):
    rows, d = inputs.shape
    width = pool_weight.shape[1]
    rwidth = query_weight.shape[1]
    heads, hk = init_state.shape[0], init_state.shape[1]
    n_sp, n_tp = lax.axis_size("sp"), lax.axis_size("tp")
    steps = n_tp
    tile = rows // steps
    d_out = out_pool.shape[1]
    n_pairs = n_sp // 2

    def rowed(w):
        return pl.BlockSpec((tile, w), lambda i: (i, 0))

    def whole(*shape):
        return pl.BlockSpec(shape, lambda i: (0,) * len(shape))

    hbm = pl.BlockSpec(memory_space=pl.ANY)
    return pl.pallas_call(
        functools.partial(layer_kernel, n_sp, n_tp, steps),
        grid=(steps,),
        in_specs=[rowed(d), whole(1, d), whole(d, width)]
        + [whole(d, rwidth)] * 4
        + [whole(1, rwidth), rowed(heads), hbm, hbm, hbm, whole(heads, hk, hk), whole(1, rwidth)]
        + [whole(*pool_mix.shape), whole(1, width)],
        out_specs=whole(tile, d_out),
        out_shape=jax.ShapeDtypeStruct((tile, d_out), BF),
        scratch_shapes=[
            pltpu.VMEM((1, rwidth), F32),
            pltpu.VMEM((heads, hk, hk), F32),
            pltpu.VMEM((rows, rwidth), F32),
            pltpu.VMEM((rows, rwidth), BF),
            pltpu.VMEM((rows, rwidth), BF),
            pltpu.VMEM((rows + HALO, width), BF),
            pltpu.VMEM((n_tp, tile, width), BF),
            pltpu.VMEM((n_tp, tile, rwidth), BF),
            pltpu.VMEM((n_tp, tile, width), BF),
            pltpu.VMEM((n_tp, tile, rwidth), BF),
            pltpu.VMEM((n_tp, width + rwidth, d_out), BF),
            pltpu.VMEM((tile, d_out), F32),
            pltpu.VMEM((HALO, d), BF),
            pltpu.VMEM((heads, hk + 16, hk), BF),
            pltpu.VMEM((heads, hk + 16, hk), BF),
            pltpu.VMEM((heads, hk + 16, hk), BF),
            pltpu.VMEM((n_pairs, heads, hk + 16, hk), BF),
            pltpu.SemaphoreType.DMA((SEMS,)),
            pltpu.SemaphoreType.DMA((SEMS,)),
            pltpu.SemaphoreType.DMA((n_pairs,)),
            pltpu.SemaphoreType.DMA((n_pairs,)),
            pltpu.SemaphoreType.DMA((2,)),
        ],
        compiler_params=pltpu.CompilerParams(
            dimension_semantics=("arbitrary",), vmem_limit_bytes=VMEM_LIMIT, collective_id=0,
            has_side_effects=True,
        ),
    )(
        inputs, norm_gain[None], pool_weight, query_weight, forget_weight, value_weight,
        outgate_weight, lower_bound[None], extra_decay, inputs[rows - HALO :], out_pool, out_recur,
        init_state, recur_gain[None], pool_mix, pool_scale[None],
    )


def solution(mesh):
    in_specs = (
        P("sp", None), P(), P(None, "tp"), P(None, "tp"), P(None, "tp"), P(None, "tp"),
        P(None, "tp"), P("tp", None, None), P("tp"), P("tp"), P("sp", "tp"), P("tp"),
        P("tp", None, None), P("tp", None), P("tp", None),
    )
    return jax.shard_map(
        per_device, mesh=mesh, in_specs=in_specs, out_specs=P(("sp", "tp"), None), check_vma=False
    )
```

time: 141 us -> 60.3 us (0.43)
  blocking collectives: 75.2 us -> 0 us
  Pallas kernels: 28.9 us -> 54 us
  between operations: 13.4 us -> 0.01 us
  matrix products: 8 us -> 0 us
  starting transfers between devices: 4.89 us -> 0 us
  other arithmetic: 4.7 us -> 0 us
    all_gather x2 -> x0, blocking collectives: 52.6 us -> none  [the longest x1 33.8 us: per_device(): sts = lax.all_gather(st.astype(BF), 'sp')]
    pallas_call x2 -> x1, Pallas kernels: 28.9 us -> 54 us  [per_device(): pl.pallas_call(functools.partial(layer_kernel, n_sp, n_tp, steps), grid=(...]
    all_to_all x1 -> x0, blocking collectives: 22.6 us -> none  [per_device(): seen = lax.all_to_all(y, 'tp', split_axis=0, concat_axis=1, tiled=True)]
    dot_general x1 -> x0, matrix products: 8 us -> none  [per_device(): return jnp.dot(seen, w_out, preferred_element_type=F32).astype(BF)]
    ppermute x1 -> x0, starting transfers between devices: 4.89 us -> none  [per_device(): lax.ppermute(pool_in[rows - HALO:], 'sp', [(i, i + 1) for i in range(n -...]
    concatenate x1 -> x0, other arithmetic: 3.15 us -> none  [per_device(): jnp.concatenate([out_pool, out_recur], axis=0)]
    unnamed x5 -> x2, local copies, waits for them, and re-layouts: 2.46 us -> 4.61 us
    all_to_all x1 -> x0, local copies, waits for them, and re-layouts: 1.89 us -> none  [per_device(): seen = lax.all_to_all(y, 'tp', split_axis=0, concat_axis=1, tiled=True)]
  transfers between devices with their start and end apart: 2 -> 0, of which waited for: 0 -> 0; matrix products, arithmetic and copies ran while one was open for 4% -> 0% of each run, Pallas kernels for 21% -> 0%
where the time goes in v1:
time: 60.3 us; the launch traced here: 60.1 us
  Pallas kernels  54 us (90%)
  local copies, waits for them, and re-layouts  6.07 us (10%)
    pallas_call x1, Pallas kernels, per_device(): pl.pallas_call(functools.partial(layer_kernel, n_sp, n_tp, steps), grid=(...  54 us
    unnamed x2, local copies, waits for them, and re-layouts  4.61 us
    slice x1, local copies, waits for them, and re-layouts, per_device(): inputs[rows - HALO:]  1.46 us

profile of v1, /device:TPU:0, one launch (start us, length us, event | category | flops | bytes accessed | tf_op | source)
XLA Modules:
  0.0 60.1 jit_solution(13988312410536130955)
XLA Ops:
  0.0 1.5 %slice.3.tail_ref = bf16[16,2048]{1,0:T(8,128)(2,1)} slice(bf16[1536,2048]{1,0:T(8,128)(2,1)} %x_ref.1), slice={[1520:1536], [0:2048]} | slice | bytes 131072 | tf_op jit(solution)/shard_map/slice | solution.py:405
  1.5 1.9 %copy.16.extra_ref = f32[1536,2]{1,0:T(8,128)} copy(f32[1536,2]{0,1:T(2,128)} %param.25) | data formatting | bytes 24576 | tf_op args[10]
  3.3 54.0 %shard_map.145 = bf16[384,2048]{1,0:T(8,128)(2,1)} custom-call(bf16[1536,2048]{1,0:T(8,128)(2,1)} %x_ref.1, f32[1,2048]{1,0:T(1,128)} %bitcast.4, bf16[2048,256]{1,0:T(8,128)(2,1)} %wp_ref.1, bf16[2048,256]{1,0:T(8,128)(2,1)} %wq_ref.1, bf16[2048,256]{1,0:T(8,128)(2,1)} %wf_ref.1, bf16[2048,256]{1,0:T(8,128)(2,1)} %wv_ref.1, bf16[2048,256]{1,0:T(8,128)(2,1)} %wo_ref.1, ...), custom_call_target="tpu_custom_call" | custom-call | tf_op jit(solution)/shard_map/pallas_call | solution.py:366
  57.4 2.7 %copy.18 = bf16[384,2048]{1,0:T(8,128)(2,1)} copy(bf16[384,2048]{1,0:T(8,128)(2,1)} %shard_map.145) | data formatting | bytes 3145728

commit v2 on v1

--- a/solution.py
+++ b/solution.py
@@ -85,7 +85,8 @@
         return w_copy(cross, 1 - par, c, SEM_G, (sp, mate))
 
     def copy_h():
-        return rdma(tail_ref, xhalo_ref, SEM_H, (following, tp))
+        rows = tail_ref.shape[0]
+        return rdma(tail_ref.at[pl.ds(rows - HALO, HALO)], xhalo_ref, SEM_H, (following, tp))
 
     def copy_s():
         return rdma(sbuf_ref, spair_ref, SEM_S, (twin, tp))
@@ -126,13 +127,6 @@
             pl.semaphore_signal(barrier, inc=1, device_id=(sp, lax.rem(tp + k, n_tp)), device_id_type=MESH)
         for k in range(1, n_sp):
             pl.semaphore_signal(barrier, inc=1, device_id=(lax.rem(sp + k, n_sp), tp), device_id_type=MESH)
-        pl.semaphore_wait(barrier, n_tp - 1 + n_sp - 1)
-        copy_h().start()
-        for copy in local_w():
-            copy.wait()
-        for c in range(PARTS):
-            copy_x(c).start()
-        copy_d().start()
         st_ref[...] = jnp.zeros_like(st_ref)
         run_ref[...] = jnp.zeros_like(run_ref)
 
@@ -161,16 +155,6 @@
             pooled = (total / reach - rows[HALO:, cols].astype(F32)).astype(BF)
             ypool_ref[index, :, cols] = (dot(pooled, mix_ref[g]) * pscale_ref[:, cols]).astype(BF)
 
-    @pl.when(step == 1)
-    def _():
-        copy_h().wait_recv()
-        halo = dot(norm(xhalo_ref[...]), wp_ref[...])
-        pin_ref[0:HALO, :] = jnp.where(sp > 0, halo, 0.0).astype(BF)
-
-    @pl.when(step > 0)
-    def _():
-        pooling(step - 1)
-
     normed = norm(x_ref[...])
     base = pl.multiple_of(step * tile, HALO)
     pin_ref[pl.ds(base + HALO, tile), :] = dot(normed, wp_ref[...]).astype(BF)
@@ -178,10 +162,31 @@
     q_raw = dot(normed, wq_ref[...])
     f_raw = dot(normed, wf_ref[...])
     value = dot(normed, wv_ref[...]).astype(BF)
+
+    @pl.when(step == 0)
+    def _():
+        pl.semaphore_wait(pltpu.get_barrier_semaphore(), n_tp - 1 + n_sp - 1)
+        copy_h().start()
+        for copy in local_w():
+            copy.wait()
+        for c in range(PARTS):
+            copy_x(c).start()
+        copy_d().start()
+
+    @pl.when(step == 1)
+    def _():
+        copy_h().wait_recv()
+        halo = dot(norm(xhalo_ref[...]), wp_ref[...])
+        pin_ref[0:HALO, :] = jnp.where(sp > 0, halo, 0.0).astype(BF)
+
+    @pl.when(step > 0)
+    def _():
+        pooling(step - 1)
+
     gap = 1.0 - lb_ref[...]
     q_in = q_raw * sigmoid(q_raw)
     k_in = gap * sigmoid(-f_raw)
-    extra = extra_ref[...]
+    extra = jnp.concatenate([extra_ref[...], jnp.zeros((8 - heads, tile), F32)], axis=0).T
     log_f = log1m(k_in) + jnp.concatenate(
         [jnp.broadcast_to(extra[:, h : h + 1], (tile, hk)) for h in range(heads)], axis=1
     )
@@ -298,6 +303,7 @@
             copy_f(c).wait_recv()
         for r in range(3):
             copy_p(r).wait_recv()
+        copy_r(2).wait_recv()
         for c in range(PARTS):
             copy_g(c).wait_recv()
         rwidth = rgot_ref.shape[2]
@@ -310,17 +316,18 @@
             acc = dot(pgot_ref[0], wg_ref[0, 0:gw, cols])
             for s in range(1, n_tp):
                 acc = acc + dot(pgot_ref[s], wg_ref[s, 0:gw, cols])
-            acc = acc + dot(rgot_ref[tp], wg_ref[tp, gw : gw + rwidth, cols])
+            for s in (tp, mate):
+                acc = acc + dot(rgot_ref[s], wg_ref[s, gw : gw + rwidth, cols])
             acc_ref[:, cols] = acc
 
-        for r in range(2, -1, -1):
+        for r in range(2):
             copy_r(r).wait_recv()
 
         @pl.loop(0, parts_out)
         def _(j):
             cols = pl.ds(pl.multiple_of(j * span, span), span)
             acc = acc_ref[:, cols]
-            for r in range(3):
+            for r in range(2):
                 s = relations[r]
                 acc = acc + dot(rgot_ref[s], wg_ref[s, gw : gw + rwidth, cols])
             out_ref[:, cols] = acc.astype(BF)
@@ -368,7 +375,7 @@
         grid=(steps,),
         in_specs=[rowed(d), whole(1, d), whole(d, width)]
         + [whole(d, rwidth)] * 4
-        + [whole(1, rwidth), rowed(heads), hbm, hbm, hbm, whole(heads, hk, hk), whole(1, rwidth)]
+        + [whole(1, rwidth), pl.BlockSpec((heads, tile), lambda i: (0, i)), hbm, hbm, hbm, whole(heads, hk, hk), whole(1, rwidth)]
         + [whole(*pool_mix.shape), whole(1, width)],
         out_specs=whole(tile, d_out),
         out_shape=jax.ShapeDtypeStruct((tile, d_out), BF),
@@ -402,7 +409,7 @@
         ),
     )(
         inputs, norm_gain[None], pool_weight, query_weight, forget_weight, value_weight,
-        outgate_weight, lower_bound[None], extra_decay, inputs[rows - HALO :], out_pool, out_recur,
+        outgate_weight, lower_bound[None], extra_decay.T, inputs, out_pool, out_recur,
         init_state, recur_gain[None], pool_mix, pool_scale[None],
     )
 

time: 60.3 us -> 56.5 us (0.937)
  local copies, waits for them, and re-layouts: 6.07 us -> 2.73 us
    unnamed x2 -> x1, local copies, waits for them, and re-layouts: 4.61 us -> 2.73 us
    slice x1 -> x0, local copies, waits for them, and re-layouts: 1.46 us -> none  [per_device(): inputs[rows - HALO:]]
where the time goes in v2:
time: 56.5 us; the launch traced here: 56.3 us
  Pallas kernels  53.6 us (95%)
  local copies, waits for them, and re-layouts  2.73 us (5%)
    pallas_call x1, Pallas kernels, per_device(): pl.pallas_call(functools.partial(layer_kernel, n_sp, n_tp, steps), grid=(...  53.6 us
    unnamed x1, local copies, waits for them, and re-layouts  2.73 us

profile of v2, /device:TPU:0, one launch (start us, length us, event | category | flops | bytes accessed | tf_op | source)
XLA Modules:
  0.0 56.3 jit_solution(7156375864684961838)
XLA Ops:
  0.0 53.6 %shard_map.145 = bf16[384,2048]{1,0:T(8,128)(2,1)} custom-call(bf16[1536,2048]{1,0:T(8,128)(2,1)} %tail_ref.1, f32[1,2048]{1,0:T(1,128)} %bitcast.6, bf16[2048,256]{1,0:T(8,128)(2,1)} %wp_ref.1, bf16[2048,256]{1,0:T(8,128)(2,1)} %wq_ref.1, bf16[2048,256]{1,0:T(8,128)(2,1)} %wf_ref.1, bf16[2048,256]{1,0:T(8,128)(2,1)} %wv_ref.1, bf16[2048,256]{1,0:T(8,128)(2,1)} %wo_ref.1, ...), custom_call_target="tpu_custom_call" | custom-call | tf_op jit(solution)/shard_map/pallas_call | solution.py:373
  53.6 2.7 %copy.17 = bf16[384,2048]{1,0:T(8,128)(2,1)} copy(bf16[384,2048]{1,0:T(8,128)(2,1)} %shard_map.145) | data formatting | bytes 3145728
